TPU v7x, 32 devices: a whole 2x2x4 slice. The times are simulated.
32 devices in a mesh: grp: 2 (over x), tp: 4 (over z), dp: 4 (over y, core).
Axes of the slice: x: 2, y: 2, z: 4, core: 2. Of those that a mesh axis runs over, the one named last changes fastest.
Arguments:
- stream: bfloat16 [32, 4096], P('grp', 'dp'), parts along dimension 0, may hold values from -11 to 11
- states: float32 [2, 32, 32, 64, 64], P(None, ('grp', 'dp'), 'tp'), parts along dimension 1, may hold values from -6 to 6
- norm_gain: bfloat16 [2, 4096], P(None, 'dp'), may hold values from 0.099609375 to 1.8984375
- recept_weight: bfloat16 [2, 4096, 2048], P(None, 'dp', 'tp'), may hold values from -0.09375 to 0.09375
- key_weight: bfloat16 [2, 4096, 2048], P(None, 'dp', 'tp'), may hold values from -0.09375 to 0.09375
- value_weight: bfloat16 [2, 4096, 2048], P(None, 'dp', 'tp'), may hold values from -0.09375 to 0.09375
- decay_weight: bfloat16 [2, 4096, 2048], P(None, 'dp', 'tp'), may hold values from -0.09375 to 0.09375
- rate_weight: bfloat16 [2, 4096, 2048], P(None, 'dp', 'tp'), may hold values from -0.09375 to 0.09375
- gate_weight: bfloat16 [2, 4096, 2048], P(None, 'dp', 'tp'), may hold values from -0.09375 to 0.09375
- out_weight: bfloat16 [2, 2048, 4096], P(None, 'tp', 'dp'), may hold values from -0.125 to 0.125
- decay_bias: float32 [2, 2048], P(None, 'tp'), may hold values from -2 to 2
- head_gain: bfloat16 [2, 2048], P(None, 'tp'), may hold values from 0.099609375 to 1.8984375
Outputs:
- new_stream: bfloat16 [32, 4096], P('grp', 'dp'), parts along dimension 0
- new_states: float32 [2, 32, 32, 64, 64], P(None, ('grp', 'dp'), 'tp'), parts along dimension 1
There are 2 independent parts, one for each index of `grp`. A program takes and returns all parts, laid end to end along the dimension named above; an argument that names none is the same for every part. Nothing has to cross between parts.
All inputs are finite; a program needn't handle non-finite values.
Results may differ from a plain program's by a relative error of at most 0.0068.
Values may be sent and summed in bfloat16 or wider, within the bound.
A program may use at most 64 MiB of HBM per device.

v0:
```python
import jax
import jax.numpy as jnp
from jax import lax
from jax.sharding import PartitionSpec as P

D = 4096
HEAD = 64


def run_block(stream, state_blk, gain, weights, out_weight, bias, hgain):
    current = stream.astype(jnp.float32)
    squares = jnp.sum(current * current, axis=1)
    normed = (current * gain.astype(jnp.float32)).astype(jnp.bfloat16)
    width = weights[0].shape[1]
    local_rows = state_blk.shape[0]
    all_totals = lax.psum(squares, "dp")
    offset = lax.axis_index("dp") * local_rows
    totals = lax.dynamic_slice_in_dim(all_totals, offset, local_rows, 0)
    summed = lax.psum_scatter(
        jnp.concatenate(
            [jnp.dot(normed, weight, preferred_element_type=jnp.float32) for weight in weights],
            axis=1,
        ),
        "dp",
        scatter_dimension=0,
        tiled=True,
    )
    inv_rms = lax.rsqrt(totals / D + 1e-06)[:, None]
    projected = (summed * inv_rms).reshape(local_rows, 6, -1, HEAD)
    recept = projected[:, 0]
    key_vec = projected[:, 1]
    value_vec = projected[:, 2]
    decay_pre = projected[:, 3]
    rate_pre = projected[:, 4]
    gate_pre = projected[:, 5]
    unit_key = key_vec * lax.rsqrt(jnp.sum(key_vec * key_vec, axis=2, keepdims=True) + 1e-06)
    rate_vec = jax.nn.sigmoid(rate_pre)
    decay = jnp.exp(-0.606531 * jax.nn.sigmoid(bias.reshape(1, -1, HEAD) + decay_pre))
    removed = jnp.einsum("bhij,bhj->bhi", state_blk, unit_key, precision=lax.Precision.HIGHEST)
    new_state = (
        state_blk * decay[:, :, None, :]
        - removed[..., None] * (unit_key * rate_vec)[:, :, None, :]
        + value_vec[..., None] * key_vec[:, :, None, :]
    )
    read = jnp.einsum("bhij,bhj->bhi", new_state, recept, precision=lax.Precision.HIGHEST)
    center = read - jnp.mean(read, axis=2, keepdims=True)
    normal_read = center * lax.rsqrt(jnp.mean(center * center, axis=2, keepdims=True) + 1e-05)
    gated = normal_read * hgain.astype(jnp.float32).reshape(1, -1, HEAD) * jax.nn.sigmoid(gate_pre)
    mixed = gated.reshape(local_rows, width).astype(jnp.bfloat16)
    branch_part = jnp.dot(
        lax.all_gather(mixed, "dp", axis=0, tiled=True),
        out_weight,
        preferred_element_type=jnp.float32,
    )
    branch = lax.psum(branch_part, "tp")
    return ((current + branch).astype(jnp.bfloat16), new_state)


def per_device(
    stream,
    states,
    norm_gain,
    recept_weight,
    key_weight,
    value_weight,
    decay_weight,
    rate_weight,
    gate_weight,
    out_weight,
    decay_bias,
    head_gain,
):
    current = stream
    fresh_list = []
    for layer in range(2):
        weights = (
            recept_weight[layer],
            key_weight[layer],
            value_weight[layer],
            decay_weight[layer],
            rate_weight[layer],
            gate_weight[layer],
        )
        current, fresh = run_block(
            current,
            states[layer],
            norm_gain[layer],
            weights,
            out_weight[layer],
            decay_bias[layer],
            head_gain[layer],
        )
        fresh_list.append(fresh)
    return (current, jnp.stack(fresh_list))


def solution(mesh):
    in_specs = (
        P("grp", "dp"),
        P(None, ("grp", "dp"), "tp", None, None),
        P(None, "dp"),
        P(None, "dp", "tp"),
        P(None, "dp", "tp"),
        P(None, "dp", "tp"),
        P(None, "dp", "tp"),
        P(None, "dp", "tp"),
        P(None, "dp", "tp"),
        P(None, "tp", "dp"),
        P(None, "tp"),
        P(None, "tp"),
    )
    out_specs = (P("grp", "dp"), P(None, ("grp", "dp"), "tp", None, None))
    return jax.shard_map(
        per_device, mesh=mesh, in_specs=in_specs, out_specs=out_specs, check_vma=False
    )
```

profile of v0, /device:TPU:0, one launch (start us, length us, event | category | flops | bytes accessed | tf_op | source)
XLA Modules:
  0.0 201.3 jit_solution(15151777179491624203)
XLA Ops:
  8.1 1.6 convolution_dynamic-update-slice_fusion.11
  9.7 1.5 convolution_dynamic-update-slice_fusion.10
  11.5 1.6 convolution_dynamic-update-slice_fusion.8
  13.4 1.5 convolution_dynamic-update-slice_fusion.6
  15.8 8.4 %psum.28 = f32[16]{0:T(128)S(1)} all-reduce(f32[16]{0:T(128)S(1)} %fusion.61), channel_id=1, replica_groups=mesh['grp'=2,'tp'=4,'dp'=4] {'dp'}, use_global_device_ids=true, to_apply=%region_2.0 | all-reduce | flops 16 | bytes 128 | tf_op jit(solution)/shard_map/psum | solution.py:16
  25.7 24.8 %all-reduce.11.cloned.1.call-done = f32[16,3072]{1,0:T(8,128)} async-done(((f32[16,3072]{1,0:T(8,128)}), f32[16,3072]{1,0:T(8,128)}) %all-reduce.11.cloned.1.call-update) | async-done | bytes 196624
  51.7 1.7 fusion.22
  53.5 2.1 %fusion.26 = f32[4,8,1,64]{3,2,1,0:T(1,128)S(1)} fusion(f32[4,8,64,1]{2,3,1,0:T(1,128)S(1)} %bitcast.192, f32[2,4,8,64,64]{4,3,2,1,0:T(8,128)S(1)} %copy-done, f32[4,8,64]{2,1,0:T(8,128)S(1)} %get-tuple-element.23, f32[4,8,64]{2,1,0:T(8,128)S(1)} %get-tuple-element.21, f32[4,8,64]{2,1,0:T(8,128)S(1)} %get-tuple-element.10, f32[4,8,64]{2,1,0:T(8,128)S(1)} %bitcast.185, ...), kind=kOutput, calls=%fused_computation.40 | convolution fusion | flops 2228224 | bytes 1155072 | tf_op jit(solution)/shard_map/bhij,bhj->bhi/dot_general | solution.py:45
  56.0 5.2 %all-gather = bf16[4,4,512]{2,1,0:T(4,128)(2,1)S(1)} all-gather(bf16[1,4,512]{2,1,0:T(4,128)(2,1)S(1)} %reshape.168), channel_id=1, replica_groups=mesh['grp'=2,'tp'=4,'dp'=4] {'dp'}, dimensions={0}, use_global_device_ids=true | all-gather | bytes 20480 | tf_op jit(solution)/shard_map/all_gather | solution.py:51
  61.2 2.1 %fusion.14 = f32[16,1024]{1,0:T(8,128)} fusion(bf16[16,512]{1,0:T(8,128)(2,1)S(1)} %reshape.169, bf16[2,512,1024]{2,1,0:T(8,128)(2,1)} %param.21), kind=kOutput, calls=%fused_computation.27 | convolution fusion | flops 16777216 | bytes 1130496 | tf_op jit(solution)/shard_map/dot_general | solution.py:50
  63.5 34.3 %all-reduce.7.cloned.1.call-done = f32[16,1024]{1,0:T(8,128)} async-done(((f32[16,1024]{1,0:T(8,128)}), f32[16,1024]{1,0:T(8,128)}) %all-reduce.7.cloned.1.call-update) | async-done | bytes 65552 | tf_op jit(solution)/shard_map/psum | solution.py:55
  98.8 5.7 %psum.30 = f32[16]{0:T(128)S(1)} all-reduce(f32[16]{0:T(128)S(1)} %get-tuple-element.8), channel_id=1, replica_groups=mesh['grp'=2,'tp'=4,'dp'=4] {'dp'}, use_global_device_ids=true, to_apply=%region_9.0 | all-reduce | flops 16 | bytes 128 | tf_op jit(solution)/shard_map/psum | solution.py:16
  104.4 1.6 convolution_dynamic-update-slice_fusion.5
  106.1 1.5 convolution_dynamic-update-slice_fusion.4
  107.8 1.5 convolution_dynamic-update-slice_fusion.2
  109.5 1.5 convolution_dynamic-update-slice_fusion
  111.8 32.0 %all-reduce.13.cloned.1.call-done = f32[16,3072]{1,0:T(8,128)} async-done(((f32[16,3072]{1,0:T(8,128)}), f32[16,3072]{1,0:T(8,128)}) %all-reduce.13.cloned.1.call-update) | async-done | bytes 196624
  145.1 1.7 fusion.8
  146.8 2.2 %multiply_add_fusion.1 = (f32[1,4,8,64,64]{4,3,2,1,0:T(8,128)S(1)}, f32[1,4,8,64,64]{4,3,2,1,0:T(8,128)}) fusion(f32[2,4,8,64,64]{4,3,2,1,0:T(8,128)S(1)} %copy-done, f32[4,8,64]{2,1,0:T(8,128)S(1)} %get-tuple-element.23, f32[4,8,64]{2,1,0:T(8,128)S(1)} %get-tuple-element.21, f32[4,8,64]{2,1,0:T(8,128)S(1)} %get-tuple-element.10, ...), kind=kLoop, calls=%fused_computation.42 | loop fusion | flops 1310720 | bytes 2179072 | tf_op jit(solution)/shard_map/add | solution.py:41
  149.0 2.1 %fusion.12 = f32[4,8,1,64]{3,2,1,0:T(1,128)S(1)} fusion(f32[4,8,64,1]{2,3,1,0:T(1,128)S(1)} %bitcast.191, f32[2,4,8,64,64]{4,3,2,1,0:T(8,128)S(1)} %copy-done, f32[4,8,64]{2,1,0:T(8,128)S(1)} %get-tuple-element.18, f32[4,8,64]{2,1,0:T(8,128)S(1)} %get-tuple-element.16, f32[4,8,64]{2,1,0:T(8,128)S(1)} %get-tuple-element.6, f32[4,8,64]{2,1,0:T(8,128)S(1)} %bitcast.188, ...), kind=kOutput, calls=%fused_computation.26 | convolution fusion | flops 2228224 | bytes 1155072 | tf_op jit(solution)/shard_map/bhij,bhj->bhi/dot_general | solution.py:45
  151.5 5.2 %all-gather.1 = bf16[4,4,512]{2,1,0:T(4,128)(2,1)S(1)} all-gather(bf16[1,4,512]{2,1,0:T(4,128)(2,1)S(1)} %reshape.170), channel_id=1, replica_groups=mesh['grp'=2,'tp'=4,'dp'=4] {'dp'}, dimensions={0}, use_global_device_ids=true | all-gather | bytes 20480 | tf_op jit(solution)/shard_map/all_gather | solution.py:51
  156.8 2.1 %fusion = f32[16,1024]{1,0:T(8,128)} fusion(bf16[16,512]{1,0:T(8,128)(2,1)S(1)} %reshape.171, bf16[2,512,1024]{2,1,0:T(8,128)(2,1)} %param.21), kind=kOutput, calls=%fused_computation.13 | convolution fusion | flops 16777216 | bytes 1130496 | tf_op jit(solution)/shard_map/dot_general | solution.py:50
  158.9 2.8 %pad_maximum_fusion = f32[2,4,8,64,64]{4,3,2,1,0:T(8,128)} fusion(f32[1,4,8,64,64]{4,3,2,1,0:T(8,128)} %get-tuple-element.13, f32[1,4,8,64,64]{4,3,2,1,0:T(8,128)S(1)} %get-tuple-element.12), kind=kLoop, calls=%fused_computation | loop fusion | flops 262144 | bytes 2097152 | tf_op jit(solution)/shard_map/stack | solution.py:94
  161.6 31.7 %all-reduce.9.cloned.1.call-done = f32[16,1024]{1,0:T(8,128)} async-done(((f32[16,1024]{1,0:T(8,128)}), f32[16,1024]{1,0:T(8,128)}) %all-reduce.9.cloned.1.call-update) | async-done | bytes 65552 | tf_op jit(solution)/shard_map/psum | solution.py:55
  (72 shorter events, 10.5 us)
Async XLA Ops:
  7.2 4.1 %copy-start.1 = (bf16[16,1024]{1,0:T(8,128)(2,1)S(1)}, bf16[16,1024]{1,0:T(8,128)(2,1)}, u32[]{:S(2)}) copy-start(bf16[16,1024]{1,0:T(8,128)(2,1)} %param.12) | copy-start | bytes 98308
  7.2 4.1 %copy-start.2 = (bf16[2,1024,512]{2,1,0:T(8,128)(2,1)S(1)}, bf16[2,1024,512]{2,1,0:T(8,128)(2,1)}, u32[]{:S(2)}) copy-start(bf16[2,1024,512]{2,1,0:T(8,128)(2,1)} %param.17) | copy-start | bytes 6291460
  7.2 43.3 %all-reduce.11.cloned.1.call-start = ((), (), s32[]{:S(2)}) async-start(), calls=%async_computation.2 | async-start | bytes 393216
  8.1 5.0 %copy-start.4 = (bf16[2,1024,512]{2,1,0:T(8,128)(2,1)S(1)}, bf16[2,1024,512]{2,1,0:T(8,128)(2,1)}, u32[]{:S(2)}) copy-start(bf16[2,1024,512]{2,1,0:T(8,128)(2,1)} %param.19) | copy-start | bytes 6291460
  11.2 12.9 %copy-start.8 = (bf16[2,512]{1,0:T(2,128)(2,1)S(1)}, bf16[2,512]{1,0:T(2,128)(2,1)}, u32[]{:S(2)}) copy-start(bf16[2,512]{1,0:T(2,128)(2,1)} %param.23) | copy-start | bytes 6148
  11.2 12.9 %copy-start.9 = (f32[2,512]{1,0:T(2,128)S(1)}, f32[2,512]{1,0:T(2,128)}, u32[]{:S(2)}) copy-start(f32[2,512]{1,0:T(2,128)} %param.22) | copy-start | bytes 12292
  11.5 12.9 %copy-start.10 = (u32[32]{0:T(128)S(1)}, u32[32]{0:T(128)}, u32[]{:S(2)}) copy-start(u32[32]{0:T(128)} %constant.34) | copy-start | bytes 388
  11.5 40.2 %copy-start = (f32[2,4,8,64,64]{4,3,2,1,0:T(8,128)S(1)}, f32[2,4,8,64,64]{4,3,2,1,0:T(8,128)}, u32[]{:S(2)}) copy-start(f32[2,4,8,64,64]{4,3,2,1,0:T(8,128)} %param.13) | copy-start | bytes 3145732
  14.9 0.7 copy-start.6
  15.6 82.2 %all-reduce.7.cloned.1.call-start = ((), (), s32[]{:S(2)}) async-start(), calls=%async_computation | async-start | bytes 131072 | tf_op jit(solution)/shard_map/psum | solution.py:55
  63.3 80.5 %all-reduce.13.cloned.1.call-start = ((), (), s32[]{:S(2)}) async-start(), calls=%async_computation.3 | async-start | bytes 393216
  104.4 3.1 %copy-start.3 = (bf16[2,1024,512]{2,1,0:T(8,128)(2,1)S(1)}, bf16[2,1024,512]{2,1,0:T(8,128)(2,1)}, u32[]{:S(2)}) copy-start(bf16[2,1024,512]{2,1,0:T(8,128)(2,1)} %param.17) | copy-start | bytes 6291460
  104.4 4.8 %copy-start.5 = (bf16[2,1024,512]{2,1,0:T(8,128)(2,1)S(1)}, bf16[2,1024,512]{2,1,0:T(8,128)(2,1)}, u32[]{:S(2)}) copy-start(bf16[2,1024,512]{2,1,0:T(8,128)(2,1)} %param.19) | copy-start | bytes 6291460
  111.0 0.7 copy-start.7
  111.7 81.6 %all-reduce.9.cloned.1.call-start = ((), (), s32[]{:S(2)}) async-start(), calls=%async_computation.1 | async-start | bytes 131072 | tf_op jit(solution)/shard_map/psum | solution.py:55
Sparse Core Ops, SparseCore 0:
  15.7 34.7 all-reduce.10
  63.5 34.3 all-reduce.6
  111.8 31.9 all-reduce.12
  159.0 34.2 all-reduce.8
where the time goes:
time: 202 us; the launch traced here: 201 us
  waiting for transfers between devices  123 us (61%)
  matrix products  25.1 us (12%)
  blocking collectives  24.5 us (12%)
  between operations  14.5 us (7%)
  other arithmetic  11.5 us (6%)
  local copies, waits for them, and re-layouts  2.74 us (1%)
    psum x2, waiting for transfers between devices, run_block(): branch = lax.psum(branch_part, 'tp')  66 us
    unnamed x6, waiting for transfers between devices  56.8 us
    psum x2, blocking collectives, run_block(): all_totals = lax.psum(squares, 'dp')  14.1 us
    dot_general x12, matrix products, run_block(): jnp.dot(normed, weight, preferred_element_type=jnp.float32)  13.3 us
    all_gather x2, blocking collectives, run_block(): lax.all_gather(mixed, 'dp', axis=0, tiled=True)  10.4 us
    dot_general x2, matrix products, run_block(): jnp.dot(lax.all_gather(mixed, 'dp', axis=0, tiled=True), out_weight, pref...  4.2 us
    dot_general x2, matrix products, run_block(): jnp.einsum('bhij,bhj->bhi', new_state, recept, precision=lax.Precision.HI...  4.16 us
  transfers between devices with their start and end apart: 4, of which 4 were waited for; matrix products, arithmetic and copies ran while one was open for 2% of the time, Pallas kernels for 0%

commit v1 on v0

--- a/solution.py
+++ b/solution.py
@@ -52,7 +52,7 @@
         out_weight,
         preferred_element_type=jnp.float32,
     )
-    branch = lax.psum(branch_part, "tp")
+    branch = jnp.sum(lax.all_gather(branch_part, "tp"), axis=0)
     return ((current + branch).astype(jnp.bfloat16), new_state)
 
 

time: 202 us -> 161 us (0.80)
  waiting for transfers between devices: 123 us -> 57.3 us
  blocking collectives: 24.5 us -> 52.7 us
  other arithmetic: 11.5 us -> 8.65 us
    psum x2 -> x0, waiting for transfers between devices: 66 us -> none  [run_block(): branch = lax.psum(branch_part, 'tp')]
    all_gather x0 -> x2, blocking collectives: none -> 28 us  [run_block(): branch = jnp.sum(lax.all_gather(branch_part, 'tp'), axis=0)]
    unnamed x6 -> x4, waiting for transfers between devices: 56.8 us -> 57.3 us
  transfers between devices with their start and end apart: 4 -> 2, of which waited for: 4 -> 2; matrix products, arithmetic and copies ran while one was open for 2% -> 1% of each run, Pallas kernels for 0% -> 0%
where the time goes in v1:
time: 161 us; the launch traced here: 160 us
  waiting for transfers between devices  57.3 us (36%)
  blocking collectives  52.7 us (33%)
  matrix products  23.9 us (15%)
  between operations  14.8 us (9%)
  other arithmetic  8.65 us (5%)
  local copies, waits for them, and re-layouts  2.75 us (2%)
    unnamed x4, waiting for transfers between devices  57.3 us
    all_gather x2, blocking collectives, run_block(): branch = jnp.sum(lax.all_gather(branch_part, 'tp'), axis=0)  28 us
    psum x2, blocking collectives, run_block(): all_totals = lax.psum(squares, 'dp')  14.3 us
    dot_general x12, matrix products, run_block(): jnp.dot(normed, weight, preferred_element_type=jnp.float32)  13.3 us
    all_gather x2, blocking collectives, run_block(): lax.all_gather(mixed, 'dp', axis=0, tiled=True)  10.4 us
    dot_general x2, matrix products, run_block(): jnp.einsum('bhij,bhj->bhi', new_state, recept, precision=lax.Precision.HI...  4.17 us
    dot_general x2, matrix products, run_block(): jnp.einsum('bhij,bhj->bhi', state_blk, unit_key, precision=lax.Precision....  3.49 us
  transfers between devices with their start and end apart: 2, of which 2 were waited for; matrix products, arithmetic and copies ran while one was open for 1% of the time, Pallas kernels for 0%

profile of v1, /device:TPU:0, one launch (start us, length us, event | category | flops | bytes accessed | tf_op | source)
XLA Modules:
  0.0 160.1 jit_solution(5820744580700640734)
XLA Ops:
  8.1 1.6 %convolution_dynamic-update-slice_fusion.11 = f32[16,3072]{1,0:T(8,128)S(1)} fusion(bf16[2,1024,512]{2,1,0:T(8,128)(2,1)} %param.15, bf16[16,1024]{1,0:T(8,128)(2,1)} %param.12, f32[1024]{0:T(1024)S(1)} %bitcast.177), kind=kOutput, calls=%fused_computation.12 | convolution fusion | flops 16826368 | bytes 1118208 | tf_op jit(solution)/shard_map/dot_general | solution.py:21
  9.7 1.5 convolution_dynamic-update-slice_fusion.10
  11.5 1.6 %convolution_dynamic-update-slice_fusion.8 = f32[16,3072]{1,0:T(8,128)S(1)} fusion(f32[16,3072]{1,0:T(8,128)S(1)} %convolution_dynamic-update-slice_fusion.9, bf16[2,1024,512]{2,1,0:T(8,128)(2,1)} %param.18, bf16[16,1024]{1,0:T(8,128)(2,1)S(1)} %copy-done.2, f32[1024]{0:T(1024)S(1)} %bitcast.180), kind=kOutput, calls=%fused_computation.9 | convolution fusion | flops 16826368 | bytes 1118208 | tf_op jit(solution)/shard_map/dot_general | solution.py:21
  13.4 1.5 convolution_dynamic-update-slice_fusion.6
  15.8 8.4 %psum.14 = f32[16]{0:T(128)S(1)} all-reduce(f32[16]{0:T(128)S(1)} %fusion.61), channel_id=1, replica_groups=mesh['grp'=2,'tp'=4,'dp'=4] {'dp'}, use_global_device_ids=true, to_apply=%region_2.0 | all-reduce | flops 16 | bytes 128 | tf_op jit(solution)/shard_map/psum | solution.py:16
  25.8 24.6 %all-reduce.5.cloned.1.call-done = f32[16,3072]{1,0:T(8,128)} async-done(((f32[16,3072]{1,0:T(8,128)}), f32[16,3072]{1,0:T(8,128)}) %all-reduce.5.cloned.1.call-update) | async-done | bytes 196624
  51.7 1.7 %fusion.22 = f32[4,8,1,64]{3,2,1,0:T(1,128)S(1)} fusion(f32[4,8,64,1]{2,3,1,0:T(1,128)S(1)} %bitcast.193, f32[2,4,8,64,64]{4,3,2,1,0:T(8,128)S(1)} %copy-done), kind=kOutput, calls=%fused_computation.35 | convolution fusion | flops 1572864 | bytes 1073152 | tf_op jit(solution)/shard_map/bhij,bhj->bhi/dot_general | solution.py:39
  53.5 2.1 %fusion.26 = f32[4,8,1,64]{3,2,1,0:T(1,128)S(1)} fusion(f32[4,8,64,1]{2,3,1,0:T(1,128)S(1)} %bitcast.196, f32[2,4,8,64,64]{4,3,2,1,0:T(8,128)S(1)} %copy-done, f32[4,8,64]{2,1,0:T(8,128)S(1)} %get-tuple-element.23, f32[4,8,64]{2,1,0:T(8,128)S(1)} %get-tuple-element.21, f32[4,8,64]{2,1,0:T(8,128)S(1)} %get-tuple-element.10, f32[4,8,64]{2,1,0:T(8,128)S(1)} %bitcast.189, ...), kind=kOutput, calls=%fused_computation.40 | convolution fusion | flops 2228224 | bytes 1155072 | tf_op jit(solution)/shard_map/bhij,bhj->bhi/dot_general | solution.py:45
  56.0 5.2 %all-gather.2 = bf16[4,4,512]{2,1,0:T(4,128)(2,1)S(1)} all-gather(bf16[1,4,512]{2,1,0:T(4,128)(2,1)S(1)} %reshape.170), channel_id=1, replica_groups=mesh['grp'=2,'tp'=4,'dp'=4] {'dp'}, dimensions={0}, use_global_device_ids=true | all-gather | bytes 20480 | tf_op jit(solution)/shard_map/all_gather | solution.py:51
  61.2 1.5 fusion.14
  62.7 14.0 %all-gather = f32[64,1024]{1,0:T(8,128)S(1)} all-gather(f32[16,1024]{1,0:T(8,128)S(1)} %fusion.14), channel_id=2, replica_groups=mesh['grp'=2,'tp'=4,'dp'=4] {'tp'}, dimensions={0}, use_global_device_ids=true | all-gather | bytes 327680 | tf_op jit(solution)/shard_map/all_gather | solution.py:55
  76.8 5.9 %psum.15 = f32[16]{0:T(128)S(1)} all-reduce(f32[16]{0:T(128)S(1)} %get-tuple-element.8), channel_id=1, replica_groups=mesh['grp'=2,'tp'=4,'dp'=4] {'dp'}, use_global_device_ids=true, to_apply=%region_9.0 | all-reduce | flops 16 | bytes 128 | tf_op jit(solution)/shard_map/psum | solution.py:16
  82.7 1.6 %convolution_dynamic-update-slice_fusion.5 = f32[16,3072]{1,0:T(8,128)S(1)} fusion(bf16[2,1024,512]{2,1,0:T(8,128)(2,1)} %param.15, bf16[16,1024]{1,0:T(8,128)(2,1)S(1)} %get-tuple-element.9, f32[1024]{0:T(1024)S(1)} %bitcast.171), kind=kOutput, calls=%fused_computation.6 | convolution fusion | flops 16826368 | bytes 1118208 | tf_op jit(solution)/shard_map/dot_general | solution.py:21
  84.3 1.5 convolution_dynamic-update-slice_fusion.4
  86.1 1.5 convolution_dynamic-update-slice_fusion.2
  87.8 1.5 convolution_dynamic-update-slice_fusion
  90.1 32.6 %all-reduce.7.cloned.1.call-done = f32[16,3072]{1,0:T(8,128)} async-done(((f32[16,3072]{1,0:T(8,128)}), f32[16,3072]{1,0:T(8,128)}) %all-reduce.7.cloned.1.call-update) | async-done | bytes 196624
  124.0 1.7 %fusion.8 = f32[4,8,1,64]{3,2,1,0:T(1,128)S(1)} fusion(f32[4,8,64,1]{2,3,1,0:T(1,128)S(1)} %bitcast.194, f32[2,4,8,64,64]{4,3,2,1,0:T(8,128)S(1)} %copy-done), kind=kOutput, calls=%fused_computation.21 | convolution fusion | flops 1572864 | bytes 1073152 | tf_op jit(solution)/shard_map/bhij,bhj->bhi/dot_general | solution.py:39
  125.7 2.2 %multiply_add_fusion.1 = (f32[1,4,8,64,64]{4,3,2,1,0:T(8,128)S(1)}, f32[1,4,8,64,64]{4,3,2,1,0:T(8,128)}) fusion(f32[2,4,8,64,64]{4,3,2,1,0:T(8,128)S(1)} %copy-done, f32[4,8,64]{2,1,0:T(8,128)S(1)} %get-tuple-element.23, f32[4,8,64]{2,1,0:T(8,128)S(1)} %get-tuple-element.21, f32[4,8,64]{2,1,0:T(8,128)S(1)} %get-tuple-element.10, ...), kind=kLoop, calls=%fused_computation.42 | loop fusion | flops 1310720 | bytes 2179072 | tf_op jit(solution)/shard_map/add | solution.py:41
  127.9 2.1 %fusion.12 = f32[4,8,1,64]{3,2,1,0:T(1,128)S(1)} fusion(f32[4,8,64,1]{2,3,1,0:T(1,128)S(1)} %bitcast.195, f32[2,4,8,64,64]{4,3,2,1,0:T(8,128)S(1)} %copy-done, f32[4,8,64]{2,1,0:T(8,128)S(1)} %get-tuple-element.18, f32[4,8,64]{2,1,0:T(8,128)S(1)} %get-tuple-element.16, f32[4,8,64]{2,1,0:T(8,128)S(1)} %get-tuple-element.6, f32[4,8,64]{2,1,0:T(8,128)S(1)} %bitcast.192, ...), kind=kOutput, calls=%fused_computation.26 | convolution fusion | flops 2228224 | bytes 1155072 | tf_op jit(solution)/shard_map/bhij,bhj->bhi/dot_general | solution.py:45
  130.4 5.2 %all-gather.3 = bf16[4,4,512]{2,1,0:T(4,128)(2,1)S(1)} all-gather(bf16[1,4,512]{2,1,0:T(4,128)(2,1)S(1)} %reshape.172), channel_id=1, replica_groups=mesh['grp'=2,'tp'=4,'dp'=4] {'dp'}, dimensions={0}, use_global_device_ids=true | all-gather | bytes 20480 | tf_op jit(solution)/shard_map/all_gather | solution.py:51
  135.6 1.5 fusion
  137.1 14.0 %all-gather.1 = f32[64,1024]{1,0:T(8,128)S(1)} all-gather(f32[16,1024]{1,0:T(8,128)S(1)} %fusion), channel_id=3, replica_groups=mesh['grp'=2,'tp'=4,'dp'=4] {'tp'}, dimensions={0}, use_global_device_ids=true | all-gather | bytes 327680 | tf_op jit(solution)/shard_map/all_gather | solution.py:55
  151.8 1.5 pad_maximum_fusion
  (72 shorter events, 8.8 us)
Async XLA Ops:
  7.2 4.1 %copy-start.2 = (bf16[16,1024]{1,0:T(8,128)(2,1)S(1)}, bf16[16,1024]{1,0:T(8,128)(2,1)}, u32[]{:S(2)}) copy-start(bf16[16,1024]{1,0:T(8,128)(2,1)} %param.12) | copy-start | bytes 98308
  7.2 4.1 %copy-start.3 = (bf16[2,1024,512]{2,1,0:T(8,128)(2,1)S(1)}, bf16[2,1024,512]{2,1,0:T(8,128)(2,1)}, u32[]{:S(2)}) copy-start(bf16[2,1024,512]{2,1,0:T(8,128)(2,1)} %param.17) | copy-start | bytes 6291460
  7.2 43.3 %all-reduce.5.cloned.1.call-start = ((), (), s32[]{:S(2)}) async-start(), calls=%async_computation | async-start | bytes 393216
  8.1 5.0 %copy-start.5 = (bf16[2,1024,512]{2,1,0:T(8,128)(2,1)S(1)}, bf16[2,1024,512]{2,1,0:T(8,128)(2,1)}, u32[]{:S(2)}) copy-start(bf16[2,1024,512]{2,1,0:T(8,128)(2,1)} %param.19) | copy-start | bytes 6291460
  11.2 12.9 %copy-start.9 = (bf16[2,512]{1,0:T(2,128)(2,1)S(1)}, bf16[2,512]{1,0:T(2,128)(2,1)}, u32[]{:S(2)}) copy-start(bf16[2,512]{1,0:T(2,128)(2,1)} %param.23) | copy-start | bytes 6148
  11.2 12.9 %copy-start.10 = (f32[2,512]{1,0:T(2,128)S(1)}, f32[2,512]{1,0:T(2,128)}, u32[]{:S(2)}) copy-start(f32[2,512]{1,0:T(2,128)} %param.22) | copy-start | bytes 12292
  11.5 13.0 %copy-start.11 = (u32[32]{0:T(128)S(1)}, u32[32]{0:T(128)}, u32[]{:S(2)}) copy-start(u32[32]{0:T(128)} %constant.34) | copy-start | bytes 388
  11.5 40.2 %copy-start = (f32[2,4,8,64,64]{4,3,2,1,0:T(8,128)S(1)}, f32[2,4,8,64,64]{4,3,2,1,0:T(8,128)}, u32[]{:S(2)}) copy-start(f32[2,4,8,64,64]{4,3,2,1,0:T(8,128)} %param.13) | copy-start | bytes 3145732
  14.9 0.7 copy-start.7
  15.6 107.1 %all-reduce.7.cloned.1.call-start = ((), (), s32[]{:S(2)}) async-start(), calls=%async_computation.1 | async-start | bytes 393216
  82.7 3.1 %copy-start.4 = (bf16[2,1024,512]{2,1,0:T(8,128)(2,1)S(1)}, bf16[2,1024,512]{2,1,0:T(8,128)(2,1)}, u32[]{:S(2)}) copy-start(bf16[2,1024,512]{2,1,0:T(8,128)(2,1)} %param.17) | copy-start | bytes 6291460
  82.7 4.8 %copy-start.6 = (bf16[2,1024,512]{2,1,0:T(8,128)(2,1)S(1)}, bf16[2,1024,512]{2,1,0:T(8,128)(2,1)}, u32[]{:S(2)}) copy-start(bf16[2,1024,512]{2,1,0:T(8,128)(2,1)} %param.19) | copy-start | bytes 6291460
  89.3 0.7 copy-start.8
  130.0 21.8 %copy-start.1 = (f32[1,4,8,64,64]{4,3,2,1,0:T(8,128)S(1)}, f32[1,4,8,64,64]{4,3,2,1,0:T(8,128)}, u32[]{:S(2)}) copy-start(f32[1,4,8,64,64]{4,3,2,1,0:T(8,128)} %get-tuple-element.13) | copy-start | bytes 1572868
Sparse Core Ops, SparseCore 0:
  15.7 34.7 all-reduce.4
  90.1 32.5 all-reduce.6
